TPU v7x, 32 devices: a whole 2x2x4 slice. The times are simulated.
32 devices in a mesh: sp: 4 (over z), fs: 4 (over y, x), tp: 2 (over core).
Axes of the slice: x: 2, y: 2, z: 4, core: 2. Of those that a mesh axis runs over, the one named last changes fastest.
Arguments:
- inputs: bfloat16 [16384, 2048], P(('fs', 'sp'), 'tp'), parts along dimension 0, may hold values from -270 to 270
- mix_gain: float32 [2048], replicated, may hold values from 0.1 to 1.9
- w_query: bfloat16 [2048, 1024], P(None, 'tp'), may hold values from -0.125 to 0.125
- w_key: bfloat16 [2048, 256], P(None, 'tp'), may hold values from -0.125 to 0.125
- w_value: bfloat16 [2048, 256], P(None, 'tp'), may hold values from -0.125 to 0.125
- query_gain: float32 [64], replicated, may hold values from 0 to 14, as said below
- key_gain: float32 [64], replicated, may hold values from 0 to 14, as said below
- sink_logit: float32 [16], P('tp'), may hold values from 3 to 7
- w_inner: bfloat16 [2048, 1024], P(None, 'tp'), may hold values from -0.125 to 0.125
- w_bmat: bfloat16 [2048, 512], P(None, 'tp'), may hold values from -0.125 to 0.125
- w_cmat: bfloat16 [2048, 512], P(None, 'tp'), may hold values from -0.125 to 0.125
- w_gate: bfloat16 [2048, 1024], P(None, 'tp'), may hold values from -0.125 to 0.125
- w_step: bfloat16 [2048, 2, 16], P(None, None, 'tp'), may hold values from -0.125 to 0.125
- conv_inner: bfloat16 [5, 1024], P(None, 'tp'), may hold values from -2.5 to 2.5
- conv_bmat: bfloat16 [5, 512], P(None, 'tp'), may hold values from -2.5 to 2.5
- conv_cmat: bfloat16 [5, 512], P(None, 'tp'), may hold values from -2.5 to 2.5
- step_bias: float32 [2, 16], P(None, 'tp'), may hold values from -1 to 1
- decay_rate: float32 [2, 16], P(None, 'tp'), may hold values from 0 to 1, as said below
- decay_offset: float32 [4096, 2, 16], P('sp', None, 'tp'), may hold values from -3 to 0, as said below
- start_state: float32 [8, 16, 64, 128], P('fs', 'tp'), parts along dimension 0, may hold values from -96 to 96
- group_gain: float32 [1024], P('tp'), may hold values from 0.1 to 1.9
- w_out_attn: bfloat16 [1024, 2048], P('tp'), may hold values from -1.5 to 1.5
- w_out_state: bfloat16 [1024, 2048], P('tp'), may hold values from -0.1875 to 0.1875
Outputs:
- mixed: bfloat16 [16384, 2048], P(('fs', 'sp', 'tp')), parts along dimension 0
There are 4 independent parts, one for each index of `fs`. A program takes and returns all parts, laid end to end along the dimension named above; an argument that names none is the same for every part. Nothing has to cross between parts.
Inputs may be any that keep to these rules, and one draw needn't show every extreme that they name: `query_gain`: positive. `key_gain`: positive. `decay_rate`: positive. `decay_offset`: never positive.
All inputs are finite; a program needn't handle non-finite values.
Results may differ from a plain program's by a relative error of at most 0.035.
Values may be sent and summed in bfloat16 or wider, within the bound.
A program may use at most 128 MiB of HBM per device.

v0:
```python
import functools

import jax
import jax.numpy as jnp
import numpy as np
from jax import lax
from jax.experimental import pallas as pl
from jax.experimental.pallas import tpu as pltpu
from jax.sharding import PartitionSpec as P

HEAD = 64
STATE = 128
CONV = 5
BLK = 128
LANE = 128
ROWS = 256
EDGE = 8

epsilon = 1e-06
rotary_base = 10000.0
F32 = jnp.float32
BF16 = jnp.bfloat16
MESH = pl.DeviceIdType.MESH


def mm(a, b):
    return jnp.dot(a, b, preferred_element_type=F32)


def mm_t(a, b):
    return lax.dot_general(a, b, (((1,), (1,)), ((), ())), preferred_element_type=F32)


def mm_hi(a, b):
    return jnp.dot(a, b, preferred_element_type=F32, precision=lax.Precision.HIGHEST)


def low_half(shape):
    return lax.broadcasted_iota(jnp.int32, shape, len(shape) - 1) < HEAD


def silu(v):
    return v / (1.0 + jnp.exp(-v))


def kernel(
    x_hbm, wq, wk, wv, wi, wb, wc, wg, ws, woa, wos,
    mix_gain, qgain, kgain, sink, taps, bias, rate, offs, start, ggain,
    cos_t, sin_t, cos_o, sin_o, expand,
    out_ref,
    w, wo, xown, xpeer, xs, rs, kv, xbuf, qb, gb, st, cb, act, gs, dec, sb, z,
    psend, precv, kvlo, kvhi, xlo, xhi, chain_s, chain_r, sem_w, sem_x, sem_xs, sem_xr,
    sem_hs, sem_hr, sem_cs, sem_cr, sem_ps, sem_pr,
    *, n_sp,
):
    me = lax.axis_index("tp")
    idx = lax.axis_index("sp")
    peer = 1 - me
    T, half = x_hbm.shape
    nb = T // BLK
    nchunk = T // ROWS
    has_prev = idx > 0
    has_next = idx < n_sp - 1

    barrier = pltpu.get_barrier_semaphore()
    pl.semaphore_signal(barrier, inc=1, device_id={"tp": peer}, device_id_type=MESH)

    @pl.when(has_prev)
    def _():
        pl.semaphore_signal(barrier, inc=1, device_id={"sp": idx - 1}, device_id_type=MESH)

    @pl.when(has_next)
    def _():
        pl.semaphore_signal(barrier, inc=1, device_id={"sp": idx + 1}, device_id_type=MESH)

    own_copies = []
    for i in range(nchunk):
        c = pltpu.make_async_copy(
            x_hbm.at[pl.ds(i * ROWS, ROWS)], xown.at[pl.ds(i * ROWS, ROWS)], sem_x.at[i]
        )
        c.start()
        own_copies.append(c)
    wcopies = []
    col = 0
    for j, src in enumerate((wk, wv, wi, wb, wc, wq, wg, ws)):
        width = src.shape[1]
        c = pltpu.make_async_copy(src, w.at[:, pl.ds(col, width)], sem_w.at[j])
        c.start()
        wcopies.append(c)
        col += width
    n_w = len(wcopies)
    na = woa.shape[0]
    oc = [
        pltpu.make_async_copy(woa, wo.at[pl.ds(0, na)], sem_w.at[n_w]),
        pltpu.make_async_copy(wos, wo.at[pl.ds(na, wos.shape[0])], sem_w.at[n_w + 1]),
    ]
    for c in oc:
        c.start()

    @pl.when(has_prev & has_next)
    def _():
        pl.semaphore_wait(barrier, 3)

    @pl.when(jnp.logical_not(has_prev & has_next))
    def _():
        pl.semaphore_wait(barrier, 2 if n_sp > 1 else 1)

    gath = []
    for i in range(nchunk):
        c = pltpu.make_async_remote_copy(
            src_ref=x_hbm.at[pl.ds(i * ROWS, ROWS)],
            dst_ref=xpeer.at[pl.ds(i * ROWS, ROWS)],
            send_sem=sem_xs.at[i],
            recv_sem=sem_xr.at[i],
            device_id={"tp": peer},
            device_id_type=MESH,
        )
        c.start()
        gath.append(c)

    gain_own = mix_gain[:, pl.ds(pl.multiple_of(me * half, LANE), half)]
    gain_peer = mix_gain[:, pl.ds(pl.multiple_of(peer * half, LANE), half)]
    for i in range(nchunk):
        own_copies[i].wait()
        gath[i].wait()

        def scale_rows(r, carry):
            rows = pl.ds(pl.multiple_of(i * ROWS + r * 32, 32), 32)
            a = xown[rows, :].astype(F32)
            b = xpeer[rows, :].astype(F32)
            total = jnp.sum(a * a + b * b, axis=1, keepdims=True)
            rs[rows, :] = jnp.broadcast_to(
                lax.rsqrt(total * (1.0 / (2 * half)) + epsilon), (32, LANE)
            )
            xs[rows, pl.ds(pl.multiple_of(me * half, LANE), half)] = (a * gain_own).astype(BF16)
            xs[rows, pl.ds(pl.multiple_of(peer * half, LANE), half)] = (b * gain_peer).astype(BF16)
            return carry

        lax.fori_loop(0, ROWS // 32, scale_rows, 0)

    co = cos_o[pl.ds(idx, 1), :]
    so = sin_o[pl.ds(idx, 1), :]

    def norm_rotate(v, gain, rows):
        shape = v.shape
        low = low_half(shape)
        sq = v * v
        s_lo = jnp.sum(jnp.where(low, sq, 0.0), axis=1, keepdims=True)
        s_hi = jnp.sum(jnp.where(low, 0.0, sq), axis=1, keepdims=True)
        v = v * lax.rsqrt(jnp.where(low, s_lo, s_hi) * (1.0 / HEAD) + epsilon) * gain
        ct = cos_t[rows, :]
        sn = sin_t[rows, :]
        cosine = co * ct - so * sn
        sine = so * ct + co * sn
        first = (lax.broadcasted_iota(jnp.int32, shape, 1) % HEAD) < HEAD // 2
        partner = jnp.where(first, -pltpu.roll(v, LANE - HEAD // 2, 1), pltpu.roll(v, HEAD // 2, 1))
        return v * cosine + partner * sine

    def row_chunk(i):
        start_row = pl.multiple_of(i * ROWS, ROWS)
        return start_row, pl.ds(start_row, ROWS)

    kvw = wk.shape[1]
    wcopies[0].wait()
    wcopies[1].wait()

    def kv_step(i, carry):
        r0, rows = row_chunk(i)
        p = mm(xs[rows, :], w[:, : 2 * kvw])
        scale = rs[rows, :]
        k = (p[:, :LANE] * scale).astype(BF16).astype(F32)
        v = (p[:, LANE:] * scale).astype(BF16).astype(F32)
        k = norm_rotate(k, kgain[...], rows)
        low = low_half(k.shape)
        k_sw = pltpu.roll(k, HEAD, 1)
        v_sw = pltpu.roll(v, HEAD, 1)
        dst = pl.ds(pl.multiple_of(r0 + BLK, BLK), ROWS)
        kv[dst, 0:LANE] = jnp.where(low, k, k_sw).astype(BF16)
        kv[dst, LANE : 2 * LANE] = jnp.where(low, k_sw, k).astype(BF16)
        kv[dst, 2 * LANE : 3 * LANE] = jnp.where(low, v, v_sw).astype(BF16)
        kv[dst, 3 * LANE : 4 * LANE] = jnp.where(low, v_sw, v).astype(BF16)
        return carry

    lax.fori_loop(0, nchunk, kv_step, 0)

    def remote(src, dst, ss, rsem, target):
        return pltpu.make_async_remote_copy(
            src_ref=src, dst_ref=dst, send_sem=ss, recv_sem=rsem,
            device_id={"sp": target}, device_id_type=MESH,
        )

    inner_w = wi.shape[1]
    state_w = wb.shape[1]
    xw = inner_w + 2 * state_w
    for j in (2, 3, 4):
        wcopies[j].wait()

    def x_step(i, carry):
        r0, rows = row_chunk(i)
        scale = rs[rows, :]
        dst = pl.ds(pl.multiple_of(r0 + EDGE, EDGE), ROWS)
        for s in range(0, xw, 256):
            p = mm(xs[rows, :], w[:, 2 * kvw + s : 2 * kvw + s + 256])
            for t in range(0, 256, LANE):
                xbuf[dst, s + t : s + t + LANE] = (p[:, t : t + LANE] * scale).astype(BF16).astype(F32)
        return carry

    kv_up = remote(kv.at[pl.ds(T, BLK)], kvlo, sem_hs.at[0], sem_hr.at[0], idx + 1)
    kv_dn = remote(kv.at[pl.ds(BLK, BLK)], kvhi, sem_hs.at[1], sem_hr.at[1], idx - 1)
    x_up = remote(xbuf.at[pl.ds(T, EDGE)], xlo, sem_hs.at[2], sem_hr.at[2], idx + 1)
    x_dn = remote(xbuf.at[pl.ds(EDGE, EDGE)], xhi, sem_hs.at[3], sem_hr.at[3], idx - 1)

    x_step(0, 0)

    @pl.when(has_next)
    def _():
        kv_up.start()

    @pl.when(has_prev)
    def _():
        kv_dn.start()

    lax.fori_loop(1, nchunk, x_step, 0)

    for j in (5, 6, 7):
        wcopies[j].wait()
    qcol = 2 * kvw + xw
    qw = wq.shape[1]
    gw = wg.shape[1]

    def q_step(i, carry):
        r0, rows = row_chunk(i)
        scale = rs[rows, :]
        xr = xs[rows, :]
        for s in range(0, qw, 256):
            p = mm(xr, w[:, qcol + s : qcol + s + 256])
            for t in range(0, 256, LANE):
                q = (p[:, t : t + LANE] * scale).astype(BF16).astype(F32)
                q = norm_rotate(q, qgain[...], rows).astype(BF16).astype(F32)
                qb[rows, s + t : s + t + LANE] = (q * HEAD ** (-0.5)).astype(BF16)
        for s in range(0, gw, 256):
            p = mm(xr, w[:, qcol + qw + s : qcol + qw + s + 256])
            for t in range(0, 256, LANE):
                gb[rows, s + t : s + t + LANE] = (p[:, t : t + LANE] * scale).astype(BF16)
        p = mm(xr, w[:, qcol + qw + gw :]) * scale + bias[...]
        step = jnp.maximum(p, 0.0) + jnp.log1p(jnp.exp(-jnp.abs(p)))
        st[rows, :] = step
        cb[rows, :] = -rate[...] * step + offs[rows, :]
        return carry

    q_step(0, 0)

    @pl.when(has_next)
    def _():
        x_up.start()

    @pl.when(has_prev)
    def _():
        x_dn.start()

    lax.fori_loop(1, nchunk, q_step, 0)

    @pl.when(has_next)
    def _():
        kv_up.wait_send()
        x_up.wait_send()
        kv_dn.wait_recv()
        x_dn.wait_recv()
        kv[pl.ds(T + BLK, BLK), :] = kvhi[...]
        xbuf[pl.ds(T + EDGE, EDGE), :] = xhi[...]

    @pl.when(jnp.logical_not(has_next))
    def _():
        kv[pl.ds(T + BLK, BLK), :] = jnp.zeros((BLK, kv.shape[1]), BF16)
        xbuf[pl.ds(T + EDGE, EDGE), :] = jnp.zeros((EDGE, xw), F32)

    @pl.when(has_prev)
    def _():
        kv_dn.wait_send()
        x_dn.wait_send()
        kv_up.wait_recv()
        x_up.wait_recv()
        kv[pl.ds(0, BLK), :] = kvlo[...]
        xbuf[pl.ds(0, EDGE), :] = xlo[...]

    @pl.when(jnp.logical_not(has_prev))
    def _():
        kv[pl.ds(0, BLK), :] = jnp.zeros((BLK, kv.shape[1]), BF16)
        xbuf[pl.ds(0, EDGE), :] = jnp.zeros((EDGE, xw), F32)

    sq = (BLK, BLK)
    ri = lax.broadcasted_iota(jnp.int32, sq, 0)
    ci = lax.broadcasted_iota(jnp.int32, sq, 1)
    heads = inner_w // HEAD
    groups = state_w // STATE
    per_group = heads // groups
    gwid = per_group * HEAD
    low = low_half(sq)

    def spread(values, column):
        return jnp.broadcast_to(values[:, column : column + 1], sq)

    def paired(values, tile, direction):
        base = direction * heads + 2 * tile
        return jnp.where(low, spread(values, base), spread(values, base + 1))

    def state_step(b, carry):
        rows = pl.ds(pl.multiple_of(b * BLK, BLK), BLK)
        lower = jnp.where(ri >= ci, 1.0, 0.0).astype(F32)
        upper = jnp.where(ri <= ci, 1.0, 0.0).astype(F32)
        d = cb[rows, :]
        c = jnp.where(ci < heads, mm_hi(lower, d), mm_hi(upper, d))
        cb[rows, :] = c
        last = jnp.where(ci[:1] < heads, c[BLK - 1 : BLK, :], c[0:1, :])
        last8 = jnp.broadcast_to(last, (8, BLK))
        wide = jnp.exp(mm_hi(last8, expand[...]))
        dec[b, 0] = wide[:, :inner_w]
        dec[b, 1] = wide[:, inner_w:]
        load = st[rows, :] * jnp.exp(last - c)
        bt = []
        for s in range(xw - LANE, -1, -LANE):
            win = xbuf[pl.ds(pl.multiple_of(b * BLK, BLK), BLK + 2 * EDGE), s : s + LANE]
            acc = jnp.zeros(sq, F32)
            for j in range(CONV):
                o = EDGE - CONV // 2 + j
                acc = acc + win[o : o + BLK] * taps[j : j + 1, s : s + LANE]
            a = silu(acc).astype(BF16)
            act[rows, s : s + LANE] = a
            if inner_w <= s < inner_w + state_w:
                bt.insert(0, a.astype(F32).T.astype(BF16))
            if s < inner_w:
                tile = s // LANE
                g = s // gwid
                af = a.astype(F32)
                for direction in range(2):
                    loaded = (af * paired(load, tile, direction)).astype(BF16)
                    gs[b, direction, :, s : s + LANE] = mm(bt[g], loaded)
        return carry

    lax.fori_loop(0, nb, state_step, 0)

    up = remote(chain_s.at[0], chain_r.at[0], sem_cs.at[0], sem_cr.at[0], idx + 1)
    dn = remote(chain_s.at[1], chain_r.at[1], sem_cs.at[1], sem_cr.at[1], idx - 1)

    def hop(direction, copy, first, has_source, has_target):
        @pl.when(has_source)
        def _():
            copy.wait_recv()

        @pl.when(has_target)
        def _():
            order = list(range(nb)) if direction == 0 else list(range(nb - 1, -1, -1))
            for s in range(0, inner_w, LANE):
                cols = slice(s, s + LANE)
                enter = jnp.where(
                    has_source, chain_r[direction, :, cols].astype(F32), start[direction, :, cols]
                )
                total = enter
                for b in order:
                    total = total * dec[b, direction, 0:1, cols] + gs[b, direction, :, cols]
                chain_s[direction, :, cols] = total.astype(BF16)

    key_w = 3 * BLK
    aj = lax.broadcasted_iota(jnp.int32, (BLK, key_w), 1)
    ai = lax.broadcasted_iota(jnp.int32, (BLK, key_w), 0)
    reach = 2 * BLK
    kv_heads = kvw // HEAD
    q_per = (qw // HEAD) // kv_heads
    ones = jnp.ones((key_w, LANE), BF16)
    turn_up = (idx * nb) // n_sp
    turn_dn = ((n_sp - 1 - idx) * nb) // n_sp

    def attend(b, carry):
        @pl.when(b == turn_up)
        def _():
            hop(0, up, idx == 0, has_prev, has_next)

        @pl.when(b == turn_dn)
        def _():
            hop(1, dn, idx == n_sp - 1, has_next, has_prev)

        rows = pl.ds(pl.multiple_of(b * BLK, BLK), BLK)
        span = pl.ds(pl.multiple_of(b * BLK, BLK), key_w)
        lo = jnp.where((idx == 0) & (b == 0), BLK, 0)
        hi = jnp.where((idx == n_sp - 1) & (b == nb - 1), 2 * BLK - 1, key_w)
        valid = (aj >= jnp.maximum(ai, lo)) & (aj <= jnp.minimum(ai + reach, hi))
        for g in range(kv_heads):
            parts = []
            for t in range(q_per // 2):
                tile = g * (q_per // 2) + t
                q = qb[rows, tile * LANE : (tile + 1) * LANE]
                zero = jnp.zeros_like(q)
                parts += [jnp.where(low, q, zero), jnp.where(low, zero, q)]
            keys = kv[span, g * LANE : (g + 1) * LANE]
            vals = kv[span, (kv_heads + g) * LANE : (kv_heads + g + 1) * LANE]
            ext = jnp.concatenate([vals, ones], axis=1)
            s_all = mm_t(jnp.concatenate(parts, axis=0), keys)
            outs = []
            for r in range(q_per):
                s = jnp.where(valid, s_all[r * BLK : (r + 1) * BLK], -1e30)
                sk = sink[g * q_per + r : g * q_per + r + 1, :]
                m = jnp.maximum(jnp.max(s, axis=1, keepdims=True), sk[:, :1])
                p = jnp.where(valid, jnp.exp(s - m), 0.0).astype(BF16)
                o = mm(p, ext)
                den = o[:, LANE:] + jnp.exp(sk - m)
                outs.append(o[:, :LANE] / den)
            for t in range(q_per // 2):
                tile = g * (q_per // 2) + t
                z[rows, tile * LANE : (tile + 1) * LANE] = jnp.where(
                    low, outs[2 * t], outs[2 * t + 1]
                ).astype(BF16)

        @pl.when((b == turn_up) & has_next)
        def _():
            up.start()

        @pl.when((b == turn_dn) & has_prev)
        def _():
            dn.start()

        return carry

    lax.fori_loop(0, nb, attend, 0)

    @pl.when(has_next)
    def _():
        up.wait_send()

    @pl.when(has_prev)
    def _():
        dn.wait_send()

    for direction in range(2):
        source = has_prev if direction == 0 else has_next
        order = list(range(nb)) if direction == 0 else list(range(nb - 1, -1, -1))
        for s in range(0, inner_w, LANE):
            cols = slice(s, s + LANE)
            total = jnp.where(
                source, chain_r[direction, :, cols].astype(F32), start[direction, :, cols]
            )
            for b in order:
                sb[b, direction, :, cols] = total.astype(BF16)
                if b != order[-1]:
                    total = total * dec[b, direction, 0:1, cols] + gs[b, direction, :, cols]

    attn_w = qw

    def mix_block(b):
        rows = pl.ds(pl.multiple_of(b * BLK, BLK), BLK)
        c = cb[rows, :]
        step = st[rows, :]
        c_t = c.T
        step_t = step.T
        diag = ri == ci
        below = ri >= ci
        for g in range(groups):
            bm = act[rows, inner_w + g * STATE : inner_w + (g + 1) * STATE]
            cm = act[rows, inner_w + state_w + g * STATE : inner_w + state_w + (g + 1) * STATE]
            scores = mm_t(cm, bm)
            carried = [mm(cm, sb[b, d, :, g * gwid : (g + 1) * gwid]) for d in range(2)]
            gated = []
            for t in range(per_group // 2):
                tile = g * (per_group // 2) + t
                ws_ = []
                cols_f, cols_b = [], []
                for u in range(2):
                    h = 2 * tile + u
                    cf = spread(c, h)
                    cr = spread(c, heads + h)
                    cols_f.append(cf)
                    cols_b.append(cr)
                    arg = jnp.where(
                        below, cf - c_t[h : h + 1, :], cr - c_t[heads + h : heads + h + 1, :]
                    )
                    sf = step_t[h : h + 1, :]
                    sr = step_t[heads + h : heads + h + 1, :]
                    fac = jnp.where(diag, sf + sr, jnp.where(below, sf, sr))
                    ws_.append((scores * jnp.exp(arg) * fac).astype(BF16))
                y = mm(jnp.concatenate(ws_, axis=0), act[rows, tile * LANE : (tile + 1) * LANE])
                y = jnp.where(low, y[:BLK], y[BLK:])
                seg = slice(t * LANE, (t + 1) * LANE)
                y = y + carried[0][:, seg] * jnp.exp(jnp.where(low, cols_f[0], cols_f[1]))
                y = y + carried[1][:, seg] * jnp.exp(jnp.where(low, cols_b[0], cols_b[1]))
                gated.append(y * silu(gb[rows, tile * LANE : (tile + 1) * LANE].astype(F32)))
            total = sum(jnp.sum(v * v, axis=1, keepdims=True) for v in gated)
            inv = lax.rsqrt(total * (1.0 / gwid) + epsilon)
            for t, v in enumerate(gated):
                s = g * gwid + t * LANE
                z[rows, attn_w + s : attn_w + s + LANE] = (
                    v * inv * ggain[:, s : s + LANE]
                ).astype(BF16)

    for c in oc:
        c.wait()
    half_rows = T // 2
    steps = half_rows // ROWS
    width = wo.shape[1]

    def mix_rows(base):
        def one(k, carry):
            mix_block(base // BLK + k)
            return carry

        lax.fori_loop(0, ROWS // BLK, one, 0)

    copies = []
    for i in range(steps):
        base = peer * half_rows + i * ROWS
        mix_rows(base)
        zr = z[pl.ds(pl.multiple_of(base, ROWS), ROWS), :]
        for s in range(0, width, 512):
            psend[i * ROWS : (i + 1) * ROWS, s : s + 512] = mm(zr, wo[:, s : s + 512]).astype(BF16)
        copies.append(
            pltpu.make_async_remote_copy(
                src_ref=psend.at[pl.ds(i * ROWS, ROWS)],
                dst_ref=precv.at[pl.ds(i * ROWS, ROWS)],
                send_sem=sem_ps.at[i],
                recv_sem=sem_pr.at[i],
                device_id={"tp": peer},
                device_id_type=MESH,
            )
        )
        if i > 0:
            copies[i - 1].start()
    for i in range(steps):
        base = me * half_rows + i * ROWS
        mix_rows(base)
        if i == 0:
            copies[-1].start()
        zr = z[pl.ds(pl.multiple_of(base, ROWS), ROWS), :]
        for s in range(0, width, 512):
            part = mm(zr, wo[:, s : s + 512]).astype(BF16).astype(F32)
            if s == 0:
                copies[i].wait()
            got = precv[i * ROWS : (i + 1) * ROWS, s : s + 512].astype(F32)
            out_ref[i * ROWS : (i + 1) * ROWS, s : s + 512] = (part + got).astype(BF16)


def tables(tokens, count):
    lane = np.arange(LANE) % (HEAD // 2)
    frequency = rotary_base ** (-lane.astype(np.float64) / (HEAD // 2))
    inner = np.arange(tokens, dtype=np.float64)[:, None] * frequency[None, :]
    outer = np.arange(count, dtype=np.float64)[:, None] * tokens * frequency[None, :]
    return [f(a).astype(np.float32) for a in (inner, outer) for f in (np.cos, np.sin)]


def local(
    n_sp,
    inputs, mix_gain, w_query, w_key, w_value, query_gain, key_gain, sink_logit,
    w_inner, w_bmat, w_cmat, w_gate, w_step, conv_inner, conv_bmat, conv_cmat,
    step_bias, decay_rate, decay_offset, start_state, group_gain, w_out_attn, w_out_state,
):
    T, half = inputs.shape
    depth = w_query.shape[0]
    heads = w_step.shape[2]
    inner_w = w_inner.shape[1]
    state_w = w_bmat.shape[1]
    xw = inner_w + 2 * state_w
    kvw = w_key.shape[1]
    qw = w_query.shape[1]
    gw = w_gate.shape[1]
    width = w_out_attn.shape[1]
    nb = T // BLK
    nchunk = T // ROWS

    def lanes(a):
        return jnp.pad(a, ((0, 0), (0, LANE - a.shape[1])))

    ws = lanes(w_step.reshape(depth, -1))
    bias = lanes(step_bias.reshape(1, -1))
    rate = lanes(decay_rate.reshape(1, -1))
    offs = lanes(decay_offset.reshape(T, -1))
    taps = jnp.concatenate([conv_inner, conv_bmat, conv_cmat], axis=1).astype(F32)
    start = start_state.reshape(2, inner_w, STATE).transpose(0, 2, 1)
    sink = jnp.broadcast_to(sink_logit[:, None], (sink_logit.shape[0], LANE))
    twice = LANE // HEAD
    ct, sn, co, so = tables(T, n_sp)
    expand = np.zeros((LANE, 2 * inner_w), np.float32)
    for c in range(2 * heads):
        expand[c, c * HEAD : (c + 1) * HEAD] = 1.0
    any_spec = pl.BlockSpec(memory_space=pl.ANY)
    vm = pl.BlockSpec(memory_space=pltpu.VMEM)
    wcols = 2 * kvw + xw + qw + gw + LANE
    V = pltpu.VMEM
    dma = pltpu.SemaphoreType.DMA
    steps = T // 2 // ROWS
    scratch = [
        V((depth, wcols), BF16),
        V((w_out_attn.shape[0] + w_out_state.shape[0], width), BF16),
        V((T, half), BF16), V((T, half), BF16), V((T, 2 * half), BF16), V((T, LANE), F32),
        V((T + 2 * BLK, 4 * LANE), BF16), V((T + 2 * EDGE, xw), F32),
        V((T, qw), BF16), V((T, gw), BF16), V((T, LANE), F32), V((T, LANE), F32),
        V((T, xw), BF16),
        V((nb, 2, STATE, inner_w), F32), V((nb, 2, 8, inner_w), F32),
        V((nb, 2, STATE, inner_w), BF16),
        V((T, qw + inner_w), BF16),
        V((T // 2, width), BF16), V((T // 2, width), BF16),
        V((BLK, 4 * LANE), BF16), V((BLK, 4 * LANE), BF16),
        V((EDGE, xw), F32), V((EDGE, xw), F32),
        V((2, STATE, inner_w), BF16), V((2, STATE, inner_w), BF16),
        dma((10,)), dma((nchunk,)), dma((nchunk,)), dma((nchunk,)),
        dma((4,)), dma((4,)), dma((2,)), dma((2,)), dma((steps,)), dma((steps,)),
    ]
    return pl.pallas_call(
        functools.partial(kernel, n_sp=n_sp),
        out_shape=jax.ShapeDtypeStruct((T // 2, width), BF16),
        in_specs=[any_spec] * 11 + [vm] * 15,
        out_specs=vm,
        scratch_shapes=scratch,
        compiler_params=pltpu.CompilerParams(
            collective_id=0, has_side_effects=True, vmem_limit_bytes=67043328
        ),
        name="mixer",
    )(
        inputs, w_query, w_key, w_value, w_inner, w_bmat, w_cmat, w_gate, ws,
        w_out_attn, w_out_state,
        mix_gain.reshape(1, -1), jnp.tile(query_gain, twice).reshape(1, -1),
        jnp.tile(key_gain, twice).reshape(1, -1), sink, taps, bias, rate, offs, start,
        group_gain.reshape(1, -1), jnp.asarray(ct), jnp.asarray(sn), jnp.asarray(co),
        jnp.asarray(so), jnp.asarray(expand),
    )


def solution(mesh):
    return jax.shard_map(
        functools.partial(local, mesh.shape["sp"]),
        mesh=mesh,
        in_specs=(
            P(("fs", "sp"), "tp"),
            P(),
            P(None, "tp"),
            P(None, "tp"),
            P(None, "tp"),
            P(),
            P(),
            P("tp"),
            P(None, "tp"),
            P(None, "tp"),
            P(None, "tp"),
            P(None, "tp"),
            P(None, None, "tp"),
            P(None, "tp"),
            P(None, "tp"),
            P(None, "tp"),
            P(None, "tp"),
            P(None, "tp"),
            P("sp", None, "tp"),
            P("fs", "tp", None, None),
            P("tp"),
            P("tp", None),
            P("tp", None),
        ),
        out_specs=P(("fs", "sp", "tp"), None),
        check_vma=False,
    )
```

profile of v0, /device:TPU:0, one launch (start us, length us, event | category | flops | bytes accessed | tf_op | source)
XLA Modules:
  0.0 86.8 jit_solution(2793717591556488449)
XLA Ops:
  0.0 0.0 copy-start
  0.0 0.8 reshape.26
  0.8 0.6 pad.16.bias
  1.4 0.8 reshape.27
  2.2 0.5 pad.17.rate
  2.7 0.7 tile.4
  3.3 0.6 reshape_tile.6.qgain
  3.9 0.7 tile.5
  4.6 0.7 reshape_tile.7.kgain
  5.2 1.3 %broadcast_in_dim.2.sink = f32[8,128]{1,0:T(8,128)} broadcast(f32[8]{0:T(128)} %param.35), dimensions={0} | broadcast | bytes 4128 | tf_op jit(solution)/shard_map/broadcast_in_dim | solution.py:575
  6.5 1.3 %maximum_convert_fusion.taps = f32[5,1024]{1,0:T(8,128)} fusion(bf16[5,256]{1,0:T(8,128)(2,1)} %param.43, bf16[5,256]{1,0:T(8,128)(2,1)} %param.42, bf16[5,512]{1,0:T(8,128)(2,1)} %param.41), kind=kLoop, calls=%fused_computation | loop fusion | flops 30720 | bytes 30720 | tf_op jit(solution)/shard_map/convert_element_type | solution.py:573
  7.9 1.1 %copy.32 = bf16[2048,16]{1,0:T(8,128)(2,1)S(1)} copy(bf16[2048,16]{0,1:T(8,128)(2,1)} %bitcast.8) | data formatting | bytes 131072 | tf_op jit(solution)/shard_map/reshape | solution.py:569
  9.0 0.9 %pad.15.ws = bf16[2048,128]{1,0:T(8,128)(2,1)} pad(bf16[2048,16]{1,0:T(8,128)(2,1)S(1)} %copy.32, bf16[]{:T(256)} %constant.13.clone.1), padding=0_0x0_112 | pad | bytes 589826 | tf_op jit(solution)/shard_map/jit(_pad)/pad | solution.py:567
  9.9 1.0 %copy.33 = f32[1024,16]{1,0:T(8,128)S(1)} copy(f32[1024,16]{0,1:T(8,128)} %bitcast.9) | data formatting | bytes 131072 | tf_op jit(solution)/shard_map/reshape | solution.py:572
  10.9 0.8 pad.18.offs
  11.8 0.0 copy-done
  11.8 1.0 %copy.34 = f32[2,512,128]{1,2,0:T(8,128)} copy(f32[2,512,128]{2,1,0:T(8,128)S(1)} %bitcast.7) | data formatting | bytes 1048576 | tf_op jit(solution)/shard_map/reshape | solution.py:574
  12.8 70.9 %mixer.1 = bf16[512,2048]{1,0:T(8,128)(2,1)} custom-call(bf16[1024,1024]{1,0:T(8,128)(2,1)} %x_hbm.1, bf16[2048,512]{1,0:T(8,128)(2,1)} %wq.1, bf16[2048,128]{1,0:T(8,128)(2,1)} %wk.1, bf16[2048,128]{1,0:T(8,128)(2,1)} %wv.1, bf16[2048,512]{1,0:T(8,128)(2,1)} %wi.1, bf16[2048,256]{1,0:T(8,128)(2,1)} %wb.1, bf16[2048,256]{1,0:T(8,128)(2,1)} %wc.1, ...), custom_call_target="tpu_custom_call" | custom-call | tf_op jit(solution)/shard_map/mixer/pallas_call | solution.py:604
  83.7 3.2 %copy.36 = bf16[512,2048]{1,0:T(8,128)(2,1)} copy(bf16[512,2048]{1,0:T(8,128)(2,1)} %mixer.1) | data formatting | bytes 4194304
Async XLA Ops:
  0.0 11.8 %copy-start = (f32[2,8,64,128]{3,2,1,0:T(8,128)S(1)}, f32[2,8,64,128]{3,2,1,0:T(8,128)}, u32[]{:S(2)}) copy-start(f32[2,8,64,128]{3,2,1,0:T(8,128)} %param.47) | copy-start | bytes 1572868
where the time goes:
time: 87.2 us; the launch traced here: 86.8 us
  Pallas kernels  70.9 us (81%)
  local copies, waits for them, and re-layouts  14.6 us (17%)
  other arithmetic  1.34 us (2%)
    pallas_call x1, Pallas kernels, local(): pl.pallas_call(functools.partial(kernel, n_sp=n_sp), out_shape=jax.ShapeD...  70.9 us
    unnamed x3, local copies, waits for them, and re-layouts  3.16 us
    pad x4, local copies, waits for them, and re-layouts, lanes(): return jnp.pad(a, ((0, 0), (0, LANE - a.shape[1])))  2.85 us

commit v1 on v0

--- a/solution.py
+++ b/solution.py
@@ -45,10 +45,10 @@
 
 def kernel(
     x_hbm, wq, wk, wv, wi, wb, wc, wg, ws, woa, wos,
-    mix_gain, qgain, kgain, sink, taps, bias, rate, offs, start, ggain,
+    mix_gain, qgain1, kgain1, sink, taps_i, taps_b, taps_c, bias2, rate2, offs, start, ggain,
     cos_t, sin_t, cos_o, sin_o, expand,
     out_ref,
-    w, wo, xown, xpeer, xs, rs, kv, xbuf, qb, gb, st, cb, act, gs, dec, sb, z,
+    w, wst, wo, xown, xpeer, xs, rs, kv, xbuf, qb, gb, st, cb, act, gs, dec, sb, z,
     psend, precv, kvlo, kvhi, xlo, xhi, chain_s, chain_r, sem_w, sem_x, sem_xs, sem_xr,
     sem_hs, sem_hr, sem_cs, sem_cr, sem_ps, sem_pr,
     *, n_sp,
@@ -84,7 +84,8 @@
     col = 0
     for j, src in enumerate((wk, wv, wi, wb, wc, wq, wg, ws)):
         width = src.shape[1]
-        c = pltpu.make_async_copy(src, w.at[:, pl.ds(col, width)], sem_w.at[j])
+        dst = w.at[:, pl.ds(col, width)] if src is not ws else wst
+        c = pltpu.make_async_copy(src, dst, sem_w.at[j])
         c.start()
         wcopies.append(c)
         col += width
@@ -96,6 +97,13 @@
     ]
     for c in oc:
         c.start()
+
+    st[...] = jnp.zeros_like(st)
+    cb[...] = jnp.zeros_like(cb)
+    qgain = jnp.concatenate([qgain1[...]] * (LANE // HEAD), axis=1)
+    kgain = jnp.concatenate([kgain1[...]] * (LANE // HEAD), axis=1)
+    bias = jnp.concatenate([bias2[0:1, :], bias2[1:2, :]], axis=1)
+    rate = jnp.concatenate([rate2[0:1, :], rate2[1:2, :]], axis=1)
 
     @pl.when(has_prev & has_next)
     def _():
@@ -170,7 +178,7 @@
         scale = rs[rows, :]
         k = (p[:, :LANE] * scale).astype(BF16).astype(F32)
         v = (p[:, LANE:] * scale).astype(BF16).astype(F32)
-        k = norm_rotate(k, kgain[...], rows)
+        k = norm_rotate(k, kgain, rows)
         low = low_half(k.shape)
         k_sw = pltpu.roll(k, HEAD, 1)
         v_sw = pltpu.roll(v, HEAD, 1)
@@ -236,16 +244,16 @@
             p = mm(xr, w[:, qcol + s : qcol + s + 256])
             for t in range(0, 256, LANE):
                 q = (p[:, t : t + LANE] * scale).astype(BF16).astype(F32)
-                q = norm_rotate(q, qgain[...], rows).astype(BF16).astype(F32)
+                q = norm_rotate(q, qgain, rows).astype(BF16).astype(F32)
                 qb[rows, s + t : s + t + LANE] = (q * HEAD ** (-0.5)).astype(BF16)
         for s in range(0, gw, 256):
             p = mm(xr, w[:, qcol + qw + s : qcol + qw + s + 256])
             for t in range(0, 256, LANE):
                 gb[rows, s + t : s + t + LANE] = (p[:, t : t + LANE] * scale).astype(BF16)
-        p = mm(xr, w[:, qcol + qw + gw :]) * scale + bias[...]
+        p = mm(xr, wst[...]) * scale[:, : wst.shape[1]] + bias
         step = jnp.maximum(p, 0.0) + jnp.log1p(jnp.exp(-jnp.abs(p)))
-        st[rows, :] = step
-        cb[rows, :] = -rate[...] * step + offs[rows, :]
+        st[rows, : wst.shape[1]] = step
+        cb[rows, : wst.shape[1]] = -rate * step + offs[rows, :]
         return carry
 
     q_step(0, 0)
@@ -319,11 +327,18 @@
         load = st[rows, :] * jnp.exp(last - c)
         bt = []
         for s in range(xw - LANE, -1, -LANE):
+            if s < inner_w:
+                tap = taps_i[:, s : s + LANE].astype(F32)
+            elif s < inner_w + state_w:
+                tap = taps_b[:, s - inner_w : s - inner_w + LANE].astype(F32)
+            else:
+                o = s - inner_w - state_w
+                tap = taps_c[:, o : o + LANE].astype(F32)
             win = xbuf[pl.ds(pl.multiple_of(b * BLK, BLK), BLK + 2 * EDGE), s : s + LANE]
             acc = jnp.zeros(sq, F32)
             for j in range(CONV):
                 o = EDGE - CONV // 2 + j
-                acc = acc + win[o : o + BLK] * taps[j : j + 1, s : s + LANE]
+                acc = acc + win[o : o + BLK] * tap[j : j + 1]
             a = silu(acc).astype(BF16)
             act[rows, s : s + LANE] = a
             if inner_w <= s < inner_w + state_w:
@@ -353,7 +368,7 @@
             for s in range(0, inner_w, LANE):
                 cols = slice(s, s + LANE)
                 enter = jnp.where(
-                    has_source, chain_r[direction, :, cols].astype(F32), start[direction, :, cols]
+                    has_source, chain_r[direction, :, cols].astype(F32), start[direction, cols, :].T
                 )
                 total = enter
                 for b in order:
@@ -398,9 +413,9 @@
             outs = []
             for r in range(q_per):
                 s = jnp.where(valid, s_all[r * BLK : (r + 1) * BLK], -1e30)
-                sk = sink[g * q_per + r : g * q_per + r + 1, :]
-                m = jnp.maximum(jnp.max(s, axis=1, keepdims=True), sk[:, :1])
-                p = jnp.where(valid, jnp.exp(s - m), 0.0).astype(BF16)
+                sk = sink[:, g * q_per + r : g * q_per + r + 1]
+                m = jnp.maximum(jnp.max(s, axis=1, keepdims=True), sk)
+                p = jnp.exp(s - m).astype(BF16)
                 o = mm(p, ext)
                 den = o[:, LANE:] + jnp.exp(sk - m)
                 outs.append(o[:, :LANE] / den)
@@ -436,7 +451,7 @@
         for s in range(0, inner_w, LANE):
             cols = slice(s, s + LANE)
             total = jnp.where(
-                source, chain_r[direction, :, cols].astype(F32), start[direction, :, cols]
+                source, chain_r[direction, :, cols].astype(F32), start[direction, cols, :].T
             )
             for b in order:
                 sb[b, direction, :, cols] = total.astype(BF16)
@@ -501,7 +516,7 @@
             mix_block(base // BLK + k)
             return carry
 
-        lax.fori_loop(0, ROWS // BLK, one, 0)
+        lax.fori_loop(0, ROWS // BLK, one, 0, unroll=True)
 
     copies = []
     for i in range(steps):
@@ -563,29 +578,21 @@
     nb = T // BLK
     nchunk = T // ROWS
 
-    def lanes(a):
-        return jnp.pad(a, ((0, 0), (0, LANE - a.shape[1])))
-
-    ws = lanes(w_step.reshape(depth, -1))
-    bias = lanes(step_bias.reshape(1, -1))
-    rate = lanes(decay_rate.reshape(1, -1))
-    offs = lanes(decay_offset.reshape(T, -1))
-    taps = jnp.concatenate([conv_inner, conv_bmat, conv_cmat], axis=1).astype(F32)
-    start = start_state.reshape(2, inner_w, STATE).transpose(0, 2, 1)
-    sink = jnp.broadcast_to(sink_logit[:, None], (sink_logit.shape[0], LANE))
-    twice = LANE // HEAD
+    ws = w_step.reshape(depth, -1)
+    offs = decay_offset.reshape(T, -1)
+    start = start_state.reshape(2, inner_w, STATE)
     ct, sn, co, so = tables(T, n_sp)
     expand = np.zeros((LANE, 2 * inner_w), np.float32)
     for c in range(2 * heads):
         expand[c, c * HEAD : (c + 1) * HEAD] = 1.0
     any_spec = pl.BlockSpec(memory_space=pl.ANY)
     vm = pl.BlockSpec(memory_space=pltpu.VMEM)
-    wcols = 2 * kvw + xw + qw + gw + LANE
+    wcols = 2 * kvw + xw + qw + gw
     V = pltpu.VMEM
     dma = pltpu.SemaphoreType.DMA
     steps = T // 2 // ROWS
     scratch = [
-        V((depth, wcols), BF16),
+        V((depth, wcols), BF16), V((depth, 2 * heads), BF16),
         V((w_out_attn.shape[0] + w_out_state.shape[0], width), BF16),
         V((T, half), BF16), V((T, half), BF16), V((T, 2 * half), BF16), V((T, LANE), F32),
         V((T + 2 * BLK, 4 * LANE), BF16), V((T + 2 * EDGE, xw), F32),
@@ -604,7 +611,7 @@
     return pl.pallas_call(
         functools.partial(kernel, n_sp=n_sp),
         out_shape=jax.ShapeDtypeStruct((T // 2, width), BF16),
-        in_specs=[any_spec] * 11 + [vm] * 15,
+        in_specs=[any_spec] * 11 + [vm] * 17,
         out_specs=vm,
         scratch_shapes=scratch,
         compiler_params=pltpu.CompilerParams(
@@ -614,8 +621,9 @@
     )(
         inputs, w_query, w_key, w_value, w_inner, w_bmat, w_cmat, w_gate, ws,
         w_out_attn, w_out_state,
-        mix_gain.reshape(1, -1), jnp.tile(query_gain, twice).reshape(1, -1),
-        jnp.tile(key_gain, twice).reshape(1, -1), sink, taps, bias, rate, offs, start,
+        mix_gain.reshape(1, -1), query_gain.reshape(1, -1), key_gain.reshape(1, -1),
+        sink_logit.reshape(1, -1), conv_inner, conv_bmat, conv_cmat, step_bias, decay_rate,
+        offs, start,
         group_gain.reshape(1, -1), jnp.asarray(ct), jnp.asarray(sn), jnp.asarray(co),
         jnp.asarray(so), jnp.asarray(expand),
     )

time: 87.2 us -> 76.4 us (0.88)
  local copies, waits for them, and re-layouts: 14.6 us -> 6.84 us
  Pallas kernels: 70.9 us -> 69.3 us
  other arithmetic: 1.34 us -> 0 us
    pad x4 -> x0, local copies, waits for them, and re-layouts: 2.85 us -> none  [lanes(): return jnp.pad(a, ((0, 0), (0, LANE - a.shape[1])))]
    another operation x4 -> x0, local copies, waits for them, and re-layouts: 2.53 us -> none  [the longest x2 1.31 us: local(): jnp.tile(key_gain, twice).reshape(1, -1)]
    pallas_call x1, Pallas kernels: 70.9 us -> 69.3 us  [local(): pl.pallas_call(functools.partial(kernel, n_sp=n_sp), out_shape=jax.ShapeD...]
    convert_element_type x1 -> x0, other arithmetic: 1.34 us -> none  [local(): jnp.concatenate([conv_inner, conv_bmat, conv_cmat], axis=1).astype(F32)]
    broadcast_in_dim x1 -> x0, local copies, waits for them, and re-layouts: 1.31 us -> none  [local(): sink = jnp.broadcast_to(sink_logit[:, None], (sink_logit.shape[0], LANE))]
    reshape x5 -> x2, local copies, waits for them, and re-layouts: 4.73 us -> 3.68 us  [the longest x1 1.84 us: local(): ws = w_step.reshape(depth, -1)]
    unnamed x3 -> x1, local copies, waits for them, and re-layouts: 3.16 us -> 3.16 us
where the time goes in v1:
time: 76.4 us; the launch traced here: 76.2 us
  Pallas kernels  69.3 us (91%)
  local copies, waits for them, and re-layouts  6.84 us (9%)
    pallas_call x1, Pallas kernels, local(): pl.pallas_call(functools.partial(kernel, n_sp=n_sp), out_shape=jax.ShapeD...  69.3 us
    unnamed x1, local copies, waits for them, and re-layouts  3.16 us
    reshape x1, local copies, waits for them, and re-layouts, local(): ws = w_step.reshape(depth, -1)  1.84 us
    reshape x1, local copies, waits for them, and re-layouts, local(): offs = decay_offset.reshape(T, -1)  1.84 us

profile of v1, /device:TPU:0, one launch (start us, length us, event | category | flops | bytes accessed | tf_op | source)
XLA Modules:
  0.0 76.2 jit_solution(9327177949304526175)
XLA Ops:
  0.0 1.8 %copy.31.ws = bf16[2048,16]{1,0:T(8,128)(2,1)} copy(bf16[2048,16]{0,1:T(8,128)(2,1)} %bitcast.9) | data formatting | bytes 131072 | tf_op jit(solution)/shard_map/reshape | solution.py:581
  1.8 1.8 %copy.32.offs = f32[1024,16]{1,0:T(8,128)} copy(f32[1024,16]{0,1:T(8,128)} %bitcast.10) | data formatting | bytes 131072 | tf_op jit(solution)/shard_map/reshape | solution.py:582
  3.7 69.3 %mixer.1 = bf16[512,2048]{1,0:T(8,128)(2,1)} custom-call(bf16[1024,1024]{1,0:T(8,128)(2,1)} %x_hbm.1, bf16[2048,512]{1,0:T(8,128)(2,1)} %wq.1, bf16[2048,128]{1,0:T(8,128)(2,1)} %wk.1, bf16[2048,128]{1,0:T(8,128)(2,1)} %wv.1, bf16[2048,512]{1,0:T(8,128)(2,1)} %wi.1, bf16[2048,256]{1,0:T(8,128)(2,1)} %wb.1, bf16[2048,256]{1,0:T(8,128)(2,1)} %wc.1, ...), custom_call_target="tpu_custom_call" | custom-call | tf_op jit(solution)/shard_map/mixer/pallas_call | solution.py:611
  73.0 3.2 %copy.34 = bf16[512,2048]{1,0:T(8,128)(2,1)} copy(bf16[512,2048]{1,0:T(8,128)(2,1)} %mixer.1) | data formatting | bytes 4194304
